TPU v7x, 256 devices: a whole 4x4x8 slice. The times are simulated.
256 devices in a mesh: sp: 32 (over z, y), tp: 8 (over x, core).
Axes of the slice: x: 4, y: 4, z: 8, core: 2. Of those that a mesh axis runs over, the one named last changes fastest.
Arguments:
- prompt: bfloat16 [4, 6144, 4096], P(None, 'sp'), may hold values from -6 to 6
- forget_weight: bfloat16 [4096, 2048], P(None, 'tp'), may hold values from -0.09375 to 0.09375
- value_weight: bfloat16 [4096, 2048], P(None, 'tp'), may hold values from -1.5 to 1.5
- lower_bound: float32 [2048], P('tp'), may hold values from 0.9 to 0.99991862
- extra_decay: float32 [4, 6144, 2048], P(None, 'sp', 'tp'), may hold values from -1.40113932 to 0
- new_token: bfloat16 [4, 4096], P(None, 'tp'), may hold values from -6 to 6
- new_query: bfloat16 [4, 2048], P(None, 'tp'), may hold values from -6 to 6
- read_gain: float32 [128], replicated, may hold values from 0.1 to 1.9
Outputs:
- state_cache: bfloat16 [128, 16, 4, 128], P('sp', 'tp')
- first_read: bfloat16 [4, 2048], P(None, 'tp')
All inputs are finite; a program needn't handle non-finite values.
Results may differ from a plain program's by a relative error of at most 0.0019.
The roundings to bfloat16 on the way count: a program that leaves them out, or rounds other values in their place, can miss the bound.
Values may be sent and summed in bfloat16 or wider, within the bound.
No kernel may reach another device: no remote copies, remote signals or barrier semaphores. Data moves between devices by JAX's collectives and lax.ppermute only.
A program may use at most 64 MiB of HBM per device.

v0:
```python
import functools

import jax
import jax.numpy as jnp
from jax import lax
from jax.experimental import pallas as pl
from jax.experimental.pallas import tpu as pltpu
from jax.sharding import PartitionSpec as P

HD = 128
TILE = 8
PIECES = 4
AHEAD = 5


def log1p_minus(key):
    poly = jnp.float32(1.0 / 7.0)
    for order in range(6, 0, -1):
        poly = poly * key + jnp.float32(1.0 / order)
    return -(key * poly)


def key_of(forget_pre, opening):
    return opening / (1.0 + jnp.exp(forget_pre))


def side_by_side(parts):
    size = HD // len(parts)
    out = parts[0]
    if len(parts) > 1:
        shape = jnp.broadcast_shapes(*(part.shape for part in parts))
        lane = lax.broadcasted_iota(jnp.int32, (*shape[:-1], HD), len(shape) - 1)
        for g in range(1, len(parts)):
            out = jnp.where(lane >= g * size, parts[g], out)
    return out


def dense_kernel(
    prompt, forget_weight, value_weight, lower_bound, extra_decay, sent,
    tokens, forget_w, value_w, extra, lower, tot, sems,
):
    seq_count, span_len, width = tokens.shape
    dests = sent.shape[0]
    head_count = forget_w.shape[1] // HD
    groups = head_count * seq_count
    per = dests // groups
    size = HD // per
    piece = width // PIECES
    groups_in = []

    def group(*pairs):
        base = sum(len(copies) for copies in groups_in)
        groups_in.append([
            pltpu.make_async_copy(source, target, sems.at[base + i])
            for i, (source, target) in enumerate(pairs)
        ])

    for p in range(PIECES):
        cut = pl.ds(p * piece, piece)
        group(
            (prompt.at[0, :, cut], tokens.at[0, :, cut]),
            (forget_weight.at[cut], forget_w.at[cut]),
            (value_weight.at[cut], value_w.at[cut]),
        )
    half = span_len // 2
    for s in range(1, seq_count):
        pairs = [
            (prompt.at[s, pl.ds(at, half)], tokens.at[s, pl.ds(at, half)]) for at in (0, half)
        ]
        if s == 1:
            pairs += [(extra_decay, extra), (lower_bound, lower)]
        group(*pairs)

    def start(at):
        if at < len(groups_in):
            for copy in groups_in[at]:
                copy.start()

    def arrive(at):
        for copy in groups_in[at]:
            copy.wait()
        start(at + AHEAD)

    for at in range(AHEAD):
        start(at)


    lane = lax.broadcasted_iota(jnp.int32, (HD, HD), 1)
    powers = [jnp.zeros((HD, HD), jnp.float32)]

    def finish(s, opening, forget_pre, values):
        key = key_of(forget_pre.astype(jnp.float32), opening)
        log_forget = log1p_minus(key) + extra[s]
        tiles = log_forget.reshape(span_len // TILE, TILE, -1)
        sub = lax.broadcasted_iota(jnp.int32, tiles.shape, 1)
        inside = jnp.where(sub < TILE - 1, pltpu.roll(tiles, TILE - 1, 1), 0.0)
        step = 1
        while step < TILE:
            inside = inside + jnp.where(sub < TILE - step, pltpu.roll(inside, TILE - step, 1), 0.0)
            step *= 2
        carry = jnp.zeros((1, log_forget.shape[1]), jnp.float32)
        beyond = []
        for at in range(span_len // TILE - 1, -1, -1):
            beyond.append(inside[at] + carry)
            carry = carry + (inside[at, :1] + tiles[at, :1])
        later = jnp.concatenate(beyond[::-1], axis=0)
        totals = carry
        weighted = (key * jnp.exp(later)).astype(jnp.bfloat16)
        for h in range(head_count):
            cut = slice(h * HD, (h + 1) * HD)
            group = h * seq_count + s
            tot[group : group + 1, :] = totals[:, cut]
            state = lax.dot_general(
                weighted[:, cut], values[:, cut], (((0,), (0,)), ((), ())),
                preferred_element_type=jnp.float32,
            )
            peak = jnp.max(jnp.abs(state), axis=1, keepdims=True)
            power = jnp.ceil(jnp.log2(jnp.maximum(peak, 1e-30)))
            state = state * jnp.exp2(-power)
            powers[0] = jnp.where(lane == group, power, powers[0])
            for c in range(per):
                turned = [
                    pltpu.roll(state[g * size : (g + 1) * size], (g - c) * size % HD, 1)
                    if g != c
                    else state[g * size : (g + 1) * size]
                    for g in range(per)
                ]
                sent[group * per + c, :size, :] = side_by_side(turned)

    forget_sum = value_sum = None
    for p in range(PIECES):
        arrive(p)
        cut = slice(p * piece, (p + 1) * piece)
        part = tokens[0, :, cut]
        forget_part = jnp.dot(part, forget_w[cut], preferred_element_type=jnp.float32)
        value_part = jnp.dot(part, value_w[cut], preferred_element_type=jnp.float32)
        forget_sum = forget_part if p == 0 else forget_sum + forget_part
        value_sum = value_part if p == 0 else value_sum + value_part
    pending = (forget_sum.astype(jnp.bfloat16), value_sum.astype(jnp.bfloat16))
    opening = None
    for s in range(1, seq_count):
        arrive(PIECES + s - 1)
        opening = 1.0 - lower[...]
        finish(s - 1, opening, *pending)
        forget_pre = jnp.dot(
            tokens[s], forget_w[...], preferred_element_type=jnp.float32
        ).astype(jnp.bfloat16)
        values = jnp.dot(
            tokens[s], value_w[...], preferred_element_type=jnp.float32
        ).astype(jnp.bfloat16)
        pending = (forget_pre, values)
    finish(seq_count - 1, opening, *pending)
    total = tot[...]
    high = total.astype(jnp.bfloat16).astype(jnp.float32)
    left = total - high
    middle = left.astype(jnp.bfloat16).astype(jnp.float32)
    parts = (powers[0].T[:groups], high, middle, left - middle)
    for k in range(dests):
        group = k // per
        for i, part in enumerate(parts):
            sent[k, size + i : size + i + 1, :] = part[group : group + 1]


def chunk_of(weight, chip, step, chips):
    rows = weight.shape[0] // chips
    source = lax.rem(chip + chips - step, chips)
    return weight.at[pl.ds(pl.multiple_of(source * rows, rows), rows)]


def token_start_kernel(
    own, pair, forget_weight, value_weight, sums, forget_w, forget_own, value_own, sems, *, axis
):
    me = lax.axis_index(axis)
    chips = forget_w.shape[0] + 1
    chip = me // 2
    copies = [
        pltpu.make_async_copy(chunk_of(forget_weight, chip, 0, chips), forget_own, sems.at[0]),
        pltpu.make_async_copy(chunk_of(value_weight, chip, 0, chips), value_own, sems.at[1]),
    ]
    for step in range(1, chips):
        copies.append(
            pltpu.make_async_copy(
                chunk_of(forget_weight, chip, step, chips), forget_w.at[step - 1],
                sems.at[step + 1],
            )
        )
    for copy in copies:
        copy.start()
    first, second = own[...].astype(jnp.float32), pair[...].astype(jnp.float32)
    even = lax.rem(me, 2) == 0
    token = jnp.concatenate(
        [jnp.where(even, first, second), jnp.where(even, second, first)], axis=1
    ).astype(jnp.bfloat16)
    for i, weight in enumerate((forget_own, value_own)):
        copies[i].wait()
        sums[i] = jnp.dot(token, weight[...], preferred_element_type=jnp.float32)
    for copy in copies[2:]:
        copy.wait()


def token_kernel(*refs, axis):
    far = refs[:-9]
    sums, forget_w, value_weight, lower_bound, new_query, reach, addend = refs[-9:-2]
    value_w, sems = refs[-2:]
    head_count = forget_w.shape[2] // HD
    me = lax.axis_index(axis)
    chips = forget_w.shape[0] + 1
    copies = [
        pltpu.make_async_copy(
            chunk_of(value_weight, me // 2, step, chips), value_w.at[step - 1], sems.at[step - 1]
        )
        for step in range(1, chips)
    ]
    for copy in copies:
        copy.start()
    even = lax.rem(me, 2) == 0
    tokens = []
    for pieces in far:
        first, second = (pieces[i].astype(jnp.float32) for i in (0, 1))
        tokens += [jnp.where(even, first, second), jnp.where(even, second, first)]
    token = jnp.concatenate(tokens, axis=1).astype(jnp.bfloat16)

    def grouped(rows):
        return jnp.concatenate([rows[:, h * HD : (h + 1) * HD] for h in range(head_count)], axis=0)

    def rounded(i, weight):
        weight = weight[...].reshape(token.shape[1], weight.shape[2])
        out = sums[i] + jnp.dot(token, weight, preferred_element_type=jnp.float32)
        return out.astype(jnp.bfloat16).astype(jnp.float32)

    new_key = key_of(rounded(0, forget_w), 1.0 - lower_bound[...])
    query = new_query[...].astype(jnp.float32)
    query = query / (1.0 + jnp.exp(-query))
    reach[...] = grouped(query * (1.0 - new_key))
    key_sum = jnp.sum(grouped(query * new_key), axis=1, keepdims=True)
    for copy in copies:
        copy.wait()
    addend[...] = key_sum * grouped(rounded(1, value_w))


def state_kernel(got, reach, shares, scales, powers, *, axis):
    blocks, _, _ = got.shape
    groups = reach.shape[0]
    per = blocks // groups
    size = HD // per
    row_share = HD // blocks
    later = jnp.zeros((1, HD), jnp.float32)
    for b in range(blocks - 1, -1, -1):
        scales[b : b + 1, :] = later
        powers[b : b + 1, :] = got[b, size : size + 1, :]
        later = later + (
            got[b, size + 1 : size + 2, :]
            + (got[b, size + 2 : size + 3, :] + got[b, size + 3 : size + 4, :])
        )
    scales[:blocks] = jnp.exp(scales[:blocks]) * jnp.exp2(powers[...])
    group = lax.axis_index(axis) // per
    scales[blocks : blocks + 1, :] = reach[pl.ds(group, 1), :]
    by_key = scales[...].T

    def spread(column):
        return side_by_side(
            [
                jnp.broadcast_to(by_key[g * size : (g + 1) * size, column : column + 1], (size, HD))
                for g in range(per)
            ]
        )

    final = None
    for b in range(blocks):
        term = spread(b) * got[b, :size, :]
        final = term if final is None else final + term
    read = jnp.sum(spread(blocks) * final, axis=0, keepdims=True)
    step = HD // 2
    while step >= size:
        read = read + pltpu.roll(jnp.broadcast_to(read, (8, HD)), step, 1)[:1]
        step //= 2
    lane = lax.broadcasted_iota(jnp.int32, (size, HD), 1)
    for g in range(per):
        turned = final if g == 0 else pltpu.roll(final, HD - g * size, 1)
        turned = jnp.where(lane < size, turned, jnp.broadcast_to(read, (size, HD)))
        for m in range(size // row_share):
            shares[g * (size // row_share) + m] = turned[m * row_share : (m + 1) * row_share]


def read_kernel(shares, addend, read_gain, state_cache, first_read, held):
    row_share, head_count, seq_count, _ = state_cache.shape
    groups = head_count * seq_count
    per, _, _ = held.shape
    size = HD // per
    for group in range(groups):
        for c in range(per):
            held[c, pl.ds(group, row_share, stride=groups), :] = shares[group * per + c]
    final = side_by_side(
        [held[c] if c == 0 else pltpu.roll(held[c], c * size, 1) for c in range(per)]
    )
    for d in range(row_share):
        for h in range(head_count):
            at = d * groups + h * seq_count
            state_cache[d, h] = final[at : at + seq_count].astype(jnp.bfloat16)
    raw = side_by_side(
        [
            held[c, :groups] if c == 1 else pltpu.roll(held[c, :groups], (c - 1) * size % HD, 1)
            for c in range(per)
        ]
    )
    raw = raw + addend[...]
    mean = jnp.mean(raw * raw, axis=1, keepdims=True)
    normed = raw * lax.rsqrt(mean + 1e-06) * read_gain[...]
    for h in range(head_count):
        first_read[:, h * HD : (h + 1) * HD] = normed[
            h * seq_count : (h + 1) * seq_count
        ].astype(jnp.bfloat16)


def near(array):
    return pltpu.with_memory_space_constraint(array, pltpu.VMEM)


def local(
    prompt, forget_weight, value_weight, lower_bound, extra_decay, new_token, new_query, read_gain
):
    seq_count, span_len, width = prompt.shape
    width_dev = forget_weight.shape[1]
    head_count = width_dev // HD
    blocks = lax.axis_size("sp")
    peers = lax.axis_size("tp")
    row_share = HD // blocks
    groups = head_count * seq_count
    rows = HD // (blocks // groups) + 8
    anywhere = pl.BlockSpec(memory_space=pltpu.HBM)
    vmem = pl.BlockSpec(memory_space=pltpu.VMEM)
    lower_row = lower_bound[None]
    pair = lax.ppermute(new_token, "tp", [(i, i ^ 1) for i in range(peers)])
    sent = pl.pallas_call(
        dense_kernel,
        out_shape=pltpu.VMEM((blocks, rows, HD), jnp.float32),
        in_specs=[anywhere] * 5,
        out_specs=vmem,
        scratch_shapes=[
            pltpu.VMEM((seq_count, span_len, width), jnp.bfloat16),
            pltpu.VMEM((width, width_dev), jnp.bfloat16),
            pltpu.VMEM((width, width_dev), jnp.bfloat16),
            pltpu.VMEM((seq_count, span_len, width_dev), jnp.float32),
            pltpu.VMEM((1, width_dev), jnp.float32),
            pltpu.VMEM((groups, HD), jnp.float32),
            pltpu.SemaphoreType.DMA((3 * PIECES + 2 * (seq_count - 1) + 2,)),
        ],
        name="dense",
    )(prompt, forget_weight, value_weight, lower_row, extra_decay)
    sent = sent.astype(jnp.float16)
    got = lax.all_to_all(sent, "sp", 0, 0, tiled=True)
    token, pair, _ = lax.optimization_barrier((new_token, pair, sent))
    both = jnp.stack([token, pair])
    far = []
    for step in range(1, peers // 2):
        far.append(lax.ppermute(both, "tp", [(i, (i + 2 * step) % peers) for i in range(peers)]))
    others = len(far)
    part = width // (others + 1)
    sums, forget_far = pl.pallas_call(
        functools.partial(token_start_kernel, axis="tp"),
        out_shape=[
            pltpu.VMEM((2, seq_count, width_dev), jnp.float32),
            pltpu.VMEM((others, part, width_dev), jnp.bfloat16),
        ],
        in_specs=[vmem, vmem, anywhere, anywhere],
        out_specs=[vmem] * 2,
        scratch_shapes=[
            pltpu.VMEM((part, width_dev), jnp.bfloat16),
            pltpu.VMEM((part, width_dev), jnp.bfloat16),
            pltpu.SemaphoreType.DMA((others + 2,)),
        ],
        name="prepare",
    )(near(token), near(pair), forget_weight, value_weight)
    reach, addend = pl.pallas_call(
        functools.partial(token_kernel, axis="tp"),
        out_shape=[pltpu.VMEM((groups, HD), jnp.float32)] * 2,
        in_specs=[vmem] * (others + 2) + [anywhere, vmem, vmem],
        out_specs=[vmem] * 2,
        scratch_shapes=[
            pltpu.VMEM((others, part, width_dev), jnp.bfloat16),
            pltpu.SemaphoreType.DMA((others,)),
        ],
        name="token",
    )(
        *map(near, far), near(sums), near(forget_far), value_weight, near(lower_row),
        near(new_query),
    )
    got = near(got.astype(jnp.float32))
    shares = pl.pallas_call(
        functools.partial(state_kernel, axis="sp"),
        out_shape=pltpu.VMEM((blocks, row_share, HD), jnp.float32),
        in_specs=[vmem, vmem],
        out_specs=vmem,
        scratch_shapes=[
            pltpu.VMEM((HD, HD), jnp.float32),
            pltpu.VMEM((blocks, HD), jnp.float32),
        ],
        name="state",
    )(got, near(reach))
    shares = near(lax.all_to_all(shares, "sp", 0, 0, tiled=True))
    state_cache, first_read = pl.pallas_call(
        read_kernel,
        out_shape=[
            jax.ShapeDtypeStruct((row_share, head_count, seq_count, HD), jnp.bfloat16),
            jax.ShapeDtypeStruct((seq_count, width_dev), jnp.bfloat16),
        ],
        in_specs=[vmem] * 3,
        out_specs=[vmem] * 2,
        scratch_shapes=[pltpu.VMEM((blocks // groups, row_share * groups, HD), jnp.float32)],
        name="read",
    )(shares, near(addend), near(read_gain[None]))
    return (state_cache, first_read)


def solution(mesh):
    return jax.shard_map(
        local,
        mesh=mesh,
        in_specs=(
            P(None, "sp", None),
            P(None, "tp"),
            P(None, "tp"),
            P("tp"),
            P(None, "sp", "tp"),
            P(None, "tp"),
            P(None, "tp"),
            P(),
        ),
        out_specs=(P("sp", "tp", None, None), P(None, "tp")),
        check_vma=False,
    )
```

profile of v0, /device:TPU:6, one launch (start us, length us, event | category | flops | bytes accessed | tf_op | source)
XLA Modules:
  0.0 53.7 jit_solution(13157464455233145511)
XLA Ops:
  0.6 0.0 copy-start
  0.6 8.0 %dense.1 = f32[32,40,128]{2,1,0:T(8,128)S(1)} custom-call(bf16[4,192,4096]{2,1,0:T(8,128)(2,1)} %prompt.1, bf16[4096,256]{1,0:T(8,128)(2,1)} %forget_weight.3, bf16[4096,256]{1,0:T(8,128)(2,1)} %refs_5_.1, f32[1,256]{1,0:T(1,128)} %bitcast.6, f32[4,192,256]{2,1,0:T(8,128)} %extra_decay.1), custom_call_target="tpu_custom_call" | custom-call | tf_op jit(solution)/shard_map/dense/pallas_call | solution.py:334
  8.6 0.8 %convert_element_type.6 = f16[32,40,128]{2,1,0:T(8,128)(2,1)} convert(f32[32,40,128]{2,1,0:T(8,128)S(1)} %dense.1) | non-fusion elementwise | flops 163840 | bytes 983040 | tf_op jit(solution)/shard_map/convert_element_type | solution.py:350
  9.4 11.5 %all-to-all-start = ((f16[32,40,128]{2,1,0:T(8,128)(2,1)}), f16[32,40,128]{2,1,0:T(8,128)(2,1)S(1)}, u32[]{:S(2)}, u32[]{:S(2)}) async-start(f16[32,40,128]{2,1,0:T(8,128)(2,1)} %convert_element_type.6), calls=%async_computation | async-start | bytes 655360 | tf_op jit(solution)/shard_map/all_to_all | solution.py:351
  20.9 0.0 copy-done
  20.9 0.1 collective-permute-start
  21.0 1.2 %collective-permute-done.pair = bf16[4,512]{1,0:T(4,128)(2,1)S(1)} collective-permute-done((bf16[4,512]{1,0:T(4,128)(2,1)S(1)}, bf16[4,512]{1,0:T(4,128)(2,1)S(1)}, u32[]{:S(2)}, u32[]{:S(2)}) %collective-permute-start) | collective-permute-done | bytes 4128 | tf_op jit(solution)/shard_map/ppermute | solution.py:333
  22.2 0.0 copy-start.1
  22.2 0.0 copy-start.2
  22.2 0.6 %collective-permute-start.1 = (bf16[2,4,512]{2,1,0:T(4,128)(2,1)S(1)}, bf16[2,4,512]{2,1,0:T(4,128)(2,1)S(1)}, u32[]{:S(2)}, u32[]{:S(2)}) collective-permute-start(bf16[2,4,512]{2,1,0:T(4,128)(2,1)S(1)} %pad_maximum_fusion), channel_id=1, source_target_pairs={{0,2},{1,3},{2,4},{3,5},{4,6},{5,7},{6,0},{7,1},{8,10},{9,11},{10,... | collective-permute-start | bytes 24584 | tf_op jit(solution)/shard_map/ppermute | solution.py:356
  22.7 2.4 %collective-permute-start.2 = (bf16[2,4,512]{2,1,0:T(4,128)(2,1)S(1)}, bf16[2,4,512]{2,1,0:T(4,128)(2,1)S(1)}, u32[]{:S(2)}, u32[]{:S(2)}) collective-permute-start(bf16[2,4,512]{2,1,0:T(4,128)(2,1)S(1)} %pad_maximum_fusion), channel_id=1, source_target_pairs={{0,4},{1,5},{2,6},{3,7},{4,0},{5,1},{6,2},{7,3},{8,12},{9,13},{10,... | collective-permute-start | bytes 24584 | tf_op jit(solution)/shard_map/ppermute | solution.py:356
  25.2 0.0 collective-permute-start.3
  25.2 1.7 %prepare.1 = (f32[2,4,256]{2,1,0:T(4,128)S(1)}, bf16[3,1024,256]{2,1,0:T(8,128)(2,1)S(1)}) custom-call(bf16[4,512]{1,0:T(4,128)(2,1)S(1)} %copy-done, bf16[4,512]{1,0:T(4,128)(2,1)S(1)} %collective-permute-done.pair, bf16[4096,256]{1,0:T(8,128)(2,1)} %forget_weight.3, bf16[4096,256]{1,0:T(8,128)(2,1)} %refs_5_.1), custom_call_target="tpu_custom_call" | custom-call | tf_op jit(solution)/shard_map/prepare/pallas_call | solution.py:359
  26.9 0.0 collective-permute-done.1.refs_0_
  26.9 1.0 %collective-permute-done.2.refs_1_ = bf16[2,4,512]{2,1,0:T(4,128)(2,1)S(1)} collective-permute-done((bf16[2,4,512]{2,1,0:T(4,128)(2,1)S(1)}, bf16[2,4,512]{2,1,0:T(4,128)(2,1)S(1)}, u32[]{:S(2)}, u32[]{:S(2)}) %collective-permute-start.2) | collective-permute-done | bytes 8224 | tf_op jit(solution)/shard_map/ppermute | solution.py:356
  27.9 2.1 %collective-permute-done.3.refs_2_ = bf16[2,4,512]{2,1,0:T(4,128)(2,1)S(1)} collective-permute-done((bf16[2,4,512]{2,1,0:T(4,128)(2,1)S(1)}, bf16[2,4,512]{2,1,0:T(4,128)(2,1)S(1)}, u32[]{:S(2)}, u32[]{:S(2)}) %collective-permute-start.3) | collective-permute-done | bytes 8224 | tf_op jit(solution)/shard_map/ppermute | solution.py:356
  30.0 0.0 copy-done.1
  30.0 0.0 copy-done.2
  30.0 0.0 copy-start.3
  30.0 2.3 %token_.1 = (f32[8,128]{1,0:T(8,128)S(1)}, f32[8,128]{1,0:T(8,128)S(1)}) custom-call(bf16[2,4,512]{2,1,0:T(4,128)(2,1)S(1)} %collective-permute-done.1.refs_0_, bf16[2,4,512]{2,1,0:T(4,128)(2,1)S(1)} %collective-permute-done.2.refs_1_, bf16[2,4,512]{2,1,0:T(4,128)(2,1)S(1)} %collective-permute-done.3.refs_2_, f32[2,4,256]{2,1,0:T(4,128)S(1)} %get-tuple-element.10.refs_3_, ...), custom_call_target="tpu_custom_call" | custom-call | tf_op jit(solution)/shard_map/token/pallas_call | solution.py:374
  32.3 2.6 %all-to-all-done = f16[32,40,128]{2,1,0:T(8,128)(2,1)S(1)} async-done(((f16[32,40,128]{2,1,0:T(8,128)(2,1)}), f16[32,40,128]{2,1,0:T(8,128)(2,1)S(1)}, u32[]{:S(2)}, u32[]{:S(2)}) %all-to-all-start) | async-done | bytes 327712 | tf_op jit(solution)/shard_map/all_to_all | solution.py:351
  35.0 1.1 %state.1 = f32[32,4,128]{2,1,0:T(4,128)S(1)} custom-call(f32[32,40,128]{2,1,0:T(8,128)S(1)} %convert_element_type.7.got, f32[8,128]{1,0:T(8,128)S(1)} %get-tuple-element.12.reach), custom_call_target="tpu_custom_call" | custom-call | tf_op jit(solution)/shard_map/state/pallas_call | solution.py:389
  36.1 16.9 %all_to_all.10.shares = f32[32,4,128]{2,1,0:T(4,128)S(1)} all-to-all(f32[32,4,128]{2,1,0:T(4,128)S(1)} %state.1), channel_id=1, replica_groups=mesh['sp'=32,'tp'=8] {'sp'}, dimensions={0} | all-to-all | bytes 131072 | tf_op jit(solution)/shard_map/all_to_all | solution.py:400
  53.0 0.0 copy-done.3
  53.0 0.8 %read.1 = (bf16[4,2,4,128]{3,2,1,0:T(4,128)(2,1)}, bf16[4,256]{1,0:T(4,128)(2,1)}) custom-call(f32[32,4,128]{2,1,0:T(4,128)S(1)} %all_to_all.10.shares, f32[8,128]{1,0:T(8,128)S(1)} %get-tuple-element.13.addend, f32[1,128]{1,0:T(1,128)S(1)} %bitcast.8), custom_call_target="tpu_custom_call" | custom-call | tf_op jit(solution)/shard_map/read/pallas_call | solution.py:401
  (2 shorter events, 0.1 us)
Async XLA Ops:
  0.6 20.3 %copy-start = (bf16[4,512]{1,0:T(4,128)(2,1)S(1)}, bf16[4,512]{1,0:T(4,128)(2,1)}, u32[]{:S(2)}) copy-start(bf16[4,512]{1,0:T(4,128)(2,1)} %own) | copy-start | bytes 12292
  9.4 25.6 %all-to-all-start = ((f16[32,40,128]{2,1,0:T(8,128)(2,1)}), f16[32,40,128]{2,1,0:T(8,128)(2,1)S(1)}, u32[]{:S(2)}, u32[]{:S(2)}) async-start(f16[32,40,128]{2,1,0:T(8,128)(2,1)} %convert_element_type.6), calls=%async_computation | async-start | bytes 655360 | tf_op jit(solution)/shard_map/all_to_all | solution.py:351
  20.9 1.3 %collective-permute-start = (bf16[4,512]{1,0:T(4,128)(2,1)S(1)}, bf16[4,512]{1,0:T(4,128)(2,1)S(1)}, u32[]{:S(2)}, u32[]{:S(2)}) collective-permute-start(bf16[4,512]{1,0:T(4,128)(2,1)S(1)} %copy-done), channel_id=1, source_target_pairs={{0,1},{1,0},{2,3},{3,2},{4,5},{5,4},{6,7},{7,6},{8,9},{9,8},{10,11... | collective-permute-start | bytes 12296 | tf_op jit(solution)/shard_map/ppermute | solution.py:333
  22.2 7.9 %copy-start.1 = (f32[256]{0:T(256)S(1)}, f32[256]{0:T(256)}, u32[]{:S(2)}) copy-start(f32[256]{0:T(256)} %param.11) | copy-start | bytes 3076
  22.2 7.9 %copy-start.2 = (bf16[4,256]{1,0:T(4,128)(2,1)S(1)}, bf16[4,256]{1,0:T(4,128)(2,1)}, u32[]{:S(2)}) copy-start(bf16[4,256]{1,0:T(4,128)(2,1)} %refs_7_.1) | copy-start | bytes 6148
  22.2 4.7 %collective-permute-start.1 = (bf16[2,4,512]{2,1,0:T(4,128)(2,1)S(1)}, bf16[2,4,512]{2,1,0:T(4,128)(2,1)S(1)}, u32[]{:S(2)}, u32[]{:S(2)}) collective-permute-start(bf16[2,4,512]{2,1,0:T(4,128)(2,1)S(1)} %pad_maximum_fusion), channel_id=1, source_target_pairs={{0,2},{1,3},{2,4},{3,5},{4,6},{5,7},{6,0},{7,1},{8,10},{9,11},{10,... | collective-permute-start | bytes 24584 | tf_op jit(solution)/shard_map/ppermute | solution.py:356
  22.7 5.2 %collective-permute-start.2 = (bf16[2,4,512]{2,1,0:T(4,128)(2,1)S(1)}, bf16[2,4,512]{2,1,0:T(4,128)(2,1)S(1)}, u32[]{:S(2)}, u32[]{:S(2)}) collective-permute-start(bf16[2,4,512]{2,1,0:T(4,128)(2,1)S(1)} %pad_maximum_fusion), channel_id=1, source_target_pairs={{0,4},{1,5},{2,6},{3,7},{4,0},{5,1},{6,2},{7,3},{8,12},{9,13},{10,... | collective-permute-start | bytes 24584 | tf_op jit(solution)/shard_map/ppermute | solution.py:356
  25.2 4.9 %collective-permute-start.3 = (bf16[2,4,512]{2,1,0:T(4,128)(2,1)S(1)}, bf16[2,4,512]{2,1,0:T(4,128)(2,1)S(1)}, u32[]{:S(2)}, u32[]{:S(2)}) collective-permute-start(bf16[2,4,512]{2,1,0:T(4,128)(2,1)S(1)} %pad_maximum_fusion), channel_id=1, source_target_pairs={{0,6},{1,7},{2,0},{3,1},{4,2},{5,3},{6,4},{7,5},{8,14},{9,15},{10,... | collective-permute-start | bytes 24584 | tf_op jit(solution)/shard_map/ppermute | solution.py:356
  30.0 22.9 %copy-start.3 = (f32[128]{0:T(128)S(1)}, f32[128]{0:T(128)}, u32[]{:S(2)}) copy-start(f32[128]{0:T(128)} %param.15) | copy-start | bytes 1540
where the time goes:
time: 54 us; the launch traced here: 53.7 us
  blocking collectives  16.9 us (31%)
  starting transfers between devices  14.6 us (27%)
  Pallas kernels  13.8 us (26%)
  waiting for transfers between devices  6.92 us (13%)
  other arithmetic  0.82 us (2%)
  between operations  0.73 us (1%)
    all_to_all x1, blocking collectives, local(): shares = near(lax.all_to_all(shares, 'sp', 0, 0, tiled=True))  16.9 us
    all_to_all x1, starting transfers between devices, local(): got = lax.all_to_all(sent, 'sp', 0, 0, tiled=True)  11.5 us
    pallas_call x1, Pallas kernels, local(): pl.pallas_call(dense_kernel, out_shape=pltpu.VMEM((blocks, rows, HD), jnp...  7.98 us
    ppermute x3, waiting for transfers between devices, local(): lax.ppermute(both, 'tp', [(i, (i + 2 * step) % peers) for i in range(peer...  3.12 us
    ppermute x3, starting transfers between devices, local(): lax.ppermute(both, 'tp', [(i, (i + 2 * step) % peers) for i in range(peer...  2.98 us
    all_to_all x1, waiting for transfers between devices, local(): got = lax.all_to_all(sent, 'sp', 0, 0, tiled=True)  2.64 us
    pallas_call x1, Pallas kernels, local(): pl.pallas_call(functools.partial(token_kernel, axis='tp'), out_shape=[plt...  2.27 us
    pallas_call x1, Pallas kernels, local(): pl.pallas_call(functools.partial(token_start_kernel, axis='tp'), out_shap...  1.72 us
  transfers between devices with their start and end apart: 5, of which 4 were waited for; matrix products, arithmetic and copies ran while one was open for 0% of the time, Pallas kernels for 7%

commit v1 on v0

--- a/solution.py
+++ b/solution.py
@@ -10,7 +10,7 @@
 HD = 128
 TILE = 8
 PIECES = 4
-AHEAD = 5
+AHEAD = 7
 
 
 def log1p_minus(key):
@@ -285,7 +285,7 @@
 def read_kernel(shares, addend, read_gain, state_cache, first_read, held):
     row_share, head_count, seq_count, _ = state_cache.shape
     groups = head_count * seq_count
-    per, _, _ = held.shape
+    per = shares.shape[0] // groups
     size = HD // per
     for group in range(groups):
         for c in range(per):
@@ -406,7 +406,7 @@
         ],
         in_specs=[vmem] * 3,
         out_specs=[vmem] * 2,
-        scratch_shapes=[pltpu.VMEM((blocks // groups, row_share * groups, HD), jnp.float32)],
+        scratch_shapes=[pltpu.VMEM((blocks // groups + 1, row_share * groups, HD), jnp.float32)],
         name="read",
     )(shares, near(addend), near(read_gain[None]))
     return (state_cache, first_read)

time: 54 us -> 54 us (level)
  no operation moved by 1% of the time
where the time goes in v1:
time: 54 us; the launch traced here: 53.7 us
  blocking collectives  16.9 us (31%)
  starting transfers between devices  14.6 us (27%)
  Pallas kernels  13.8 us (26%)
  waiting for transfers between devices  6.92 us (13%)
  other arithmetic  0.82 us (2%)
  between operations  0.73 us (1%)
    all_to_all x1, blocking collectives, local(): shares = near(lax.all_to_all(shares, 'sp', 0, 0, tiled=True))  16.9 us
    all_to_all x1, starting transfers between devices, local(): got = lax.all_to_all(sent, 'sp', 0, 0, tiled=True)  11.5 us
    pallas_call x1, Pallas kernels, local(): pl.pallas_call(dense_kernel, out_shape=pltpu.VMEM((blocks, rows, HD), jnp...  7.98 us
    ppermute x3, waiting for transfers between devices, local(): lax.ppermute(both, 'tp', [(i, (i + 2 * step) % peers) for i in range(peer...  3.12 us
    ppermute x3, starting transfers between devices, local(): lax.ppermute(both, 'tp', [(i, (i + 2 * step) % peers) for i in range(peer...  2.98 us
    all_to_all x1, waiting for transfers between devices, local(): got = lax.all_to_all(sent, 'sp', 0, 0, tiled=True)  2.64 us
    pallas_call x1, Pallas kernels, local(): pl.pallas_call(functools.partial(token_kernel, axis='tp'), out_shape=[plt...  2.27 us
    pallas_call x1, Pallas kernels, local(): pl.pallas_call(functools.partial(token_start_kernel, axis='tp'), out_shap...  1.72 us
  transfers between devices with their start and end apart: 5, of which 4 were waited for; matrix products, arithmetic and copies ran while one was open for 0% of the time, Pallas kernels for 7%

profile of v1, /device:TPU:6, one launch (start us, length us, event | category | flops | bytes accessed | tf_op | source)
XLA Modules:
  0.0 53.7 jit_solution(9873376554298561191)
XLA Ops:
  0.6 0.0 copy-start
  0.6 8.0 %dense.1 = f32[32,40,128]{2,1,0:T(8,128)S(1)} custom-call(bf16[4,192,4096]{2,1,0:T(8,128)(2,1)} %prompt.1, bf16[4096,256]{1,0:T(8,128)(2,1)} %forget_weight.3, bf16[4096,256]{1,0:T(8,128)(2,1)} %refs_5_.1, f32[1,256]{1,0:T(1,128)} %bitcast.6, f32[4,192,256]{2,1,0:T(8,128)} %extra_decay.1), custom_call_target="tpu_custom_call" | custom-call | tf_op jit(solution)/shard_map/dense/pallas_call | solution.py:334
  8.6 0.8 %convert_element_type.6 = f16[32,40,128]{2,1,0:T(8,128)(2,1)} convert(f32[32,40,128]{2,1,0:T(8,128)S(1)} %dense.1) | non-fusion elementwise | flops 163840 | bytes 983040 | tf_op jit(solution)/shard_map/convert_element_type | solution.py:350
  9.4 11.5 %all-to-all-start = ((f16[32,40,128]{2,1,0:T(8,128)(2,1)}), f16[32,40,128]{2,1,0:T(8,128)(2,1)S(1)}, u32[]{:S(2)}, u32[]{:S(2)}) async-start(f16[32,40,128]{2,1,0:T(8,128)(2,1)} %convert_element_type.6), calls=%async_computation | async-start | bytes 655360 | tf_op jit(solution)/shard_map/all_to_all | solution.py:351
  20.9 0.0 copy-done
  20.9 0.1 collective-permute-start
  21.0 1.2 %collective-permute-done.pair = bf16[4,512]{1,0:T(4,128)(2,1)S(1)} collective-permute-done((bf16[4,512]{1,0:T(4,128)(2,1)S(1)}, bf16[4,512]{1,0:T(4,128)(2,1)S(1)}, u32[]{:S(2)}, u32[]{:S(2)}) %collective-permute-start) | collective-permute-done | bytes 4128 | tf_op jit(solution)/shard_map/ppermute | solution.py:333
  22.2 0.0 copy-start.1
  22.2 0.0 copy-start.2
  22.2 0.6 %collective-permute-start.1 = (bf16[2,4,512]{2,1,0:T(4,128)(2,1)S(1)}, bf16[2,4,512]{2,1,0:T(4,128)(2,1)S(1)}, u32[]{:S(2)}, u32[]{:S(2)}) collective-permute-start(bf16[2,4,512]{2,1,0:T(4,128)(2,1)S(1)} %pad_maximum_fusion), channel_id=1, source_target_pairs={{0,2},{1,3},{2,4},{3,5},{4,6},{5,7},{6,0},{7,1},{8,10},{9,11},{10,... | collective-permute-start | bytes 24584 | tf_op jit(solution)/shard_map/ppermute | solution.py:356
  22.7 2.4 %collective-permute-start.2 = (bf16[2,4,512]{2,1,0:T(4,128)(2,1)S(1)}, bf16[2,4,512]{2,1,0:T(4,128)(2,1)S(1)}, u32[]{:S(2)}, u32[]{:S(2)}) collective-permute-start(bf16[2,4,512]{2,1,0:T(4,128)(2,1)S(1)} %pad_maximum_fusion), channel_id=1, source_target_pairs={{0,4},{1,5},{2,6},{3,7},{4,0},{5,1},{6,2},{7,3},{8,12},{9,13},{10,... | collective-permute-start | bytes 24584 | tf_op jit(solution)/shard_map/ppermute | solution.py:356
  25.2 0.0 collective-permute-start.3
  25.2 1.7 %prepare.1 = (f32[2,4,256]{2,1,0:T(4,128)S(1)}, bf16[3,1024,256]{2,1,0:T(8,128)(2,1)S(1)}) custom-call(bf16[4,512]{1,0:T(4,128)(2,1)S(1)} %copy-done, bf16[4,512]{1,0:T(4,128)(2,1)S(1)} %collective-permute-done.pair, bf16[4096,256]{1,0:T(8,128)(2,1)} %forget_weight.3, bf16[4096,256]{1,0:T(8,128)(2,1)} %refs_5_.1), custom_call_target="tpu_custom_call" | custom-call | tf_op jit(solution)/shard_map/prepare/pallas_call | solution.py:359
  26.9 0.0 collective-permute-done.1.refs_0_
  26.9 1.0 %collective-permute-done.2.refs_1_ = bf16[2,4,512]{2,1,0:T(4,128)(2,1)S(1)} collective-permute-done((bf16[2,4,512]{2,1,0:T(4,128)(2,1)S(1)}, bf16[2,4,512]{2,1,0:T(4,128)(2,1)S(1)}, u32[]{:S(2)}, u32[]{:S(2)}) %collective-permute-start.2) | collective-permute-done | bytes 8224 | tf_op jit(solution)/shard_map/ppermute | solution.py:356
  27.9 2.1 %collective-permute-done.3.refs_2_ = bf16[2,4,512]{2,1,0:T(4,128)(2,1)S(1)} collective-permute-done((bf16[2,4,512]{2,1,0:T(4,128)(2,1)S(1)}, bf16[2,4,512]{2,1,0:T(4,128)(2,1)S(1)}, u32[]{:S(2)}, u32[]{:S(2)}) %collective-permute-start.3) | collective-permute-done | bytes 8224 | tf_op jit(solution)/shard_map/ppermute | solution.py:356
  30.0 0.0 copy-done.1
  30.0 0.0 copy-done.2
  30.0 0.0 copy-start.3
  30.0 2.3 %token_.1 = (f32[8,128]{1,0:T(8,128)S(1)}, f32[8,128]{1,0:T(8,128)S(1)}) custom-call(bf16[2,4,512]{2,1,0:T(4,128)(2,1)S(1)} %collective-permute-done.1.refs_0_, bf16[2,4,512]{2,1,0:T(4,128)(2,1)S(1)} %collective-permute-done.2.refs_1_, bf16[2,4,512]{2,1,0:T(4,128)(2,1)S(1)} %collective-permute-done.3.refs_2_, f32[2,4,256]{2,1,0:T(4,128)S(1)} %get-tuple-element.10.refs_3_, ...), custom_call_target="tpu_custom_call" | custom-call | tf_op jit(solution)/shard_map/token/pallas_call | solution.py:374
  32.3 2.6 %all-to-all-done = f16[32,40,128]{2,1,0:T(8,128)(2,1)S(1)} async-done(((f16[32,40,128]{2,1,0:T(8,128)(2,1)}), f16[32,40,128]{2,1,0:T(8,128)(2,1)S(1)}, u32[]{:S(2)}, u32[]{:S(2)}) %all-to-all-start) | async-done | bytes 327712 | tf_op jit(solution)/shard_map/all_to_all | solution.py:351
  35.0 1.1 %state.1 = f32[32,4,128]{2,1,0:T(4,128)S(1)} custom-call(f32[32,40,128]{2,1,0:T(8,128)S(1)} %convert_element_type.7.got, f32[8,128]{1,0:T(8,128)S(1)} %get-tuple-element.12.reach), custom_call_target="tpu_custom_call" | custom-call | tf_op jit(solution)/shard_map/state/pallas_call | solution.py:389
  36.1 16.9 %all_to_all.10.shares = f32[32,4,128]{2,1,0:T(4,128)S(1)} all-to-all(f32[32,4,128]{2,1,0:T(4,128)S(1)} %state.1), channel_id=1, replica_groups=mesh['sp'=32,'tp'=8] {'sp'}, dimensions={0} | all-to-all | bytes 131072 | tf_op jit(solution)/shard_map/all_to_all | solution.py:400
  53.0 0.0 copy-done.3
  53.0 0.8 %read.1 = (bf16[4,2,4,128]{3,2,1,0:T(4,128)(2,1)}, bf16[4,256]{1,0:T(4,128)(2,1)}) custom-call(f32[32,4,128]{2,1,0:T(4,128)S(1)} %all_to_all.10.shares, f32[8,128]{1,0:T(8,128)S(1)} %get-tuple-element.13.addend, f32[1,128]{1,0:T(1,128)S(1)} %bitcast.8), custom_call_target="tpu_custom_call" | custom-call | tf_op jit(solution)/shard_map/read/pallas_call | solution.py:401
  (2 shorter events, 0.1 us)
Async XLA Ops:
  0.6 20.3 %copy-start = (bf16[4,512]{1,0:T(4,128)(2,1)S(1)}, bf16[4,512]{1,0:T(4,128)(2,1)}, u32[]{:S(2)}) copy-start(bf16[4,512]{1,0:T(4,128)(2,1)} %own) | copy-start | bytes 12292
  9.4 25.6 %all-to-all-start = ((f16[32,40,128]{2,1,0:T(8,128)(2,1)}), f16[32,40,128]{2,1,0:T(8,128)(2,1)S(1)}, u32[]{:S(2)}, u32[]{:S(2)}) async-start(f16[32,40,128]{2,1,0:T(8,128)(2,1)} %convert_element_type.6), calls=%async_computation | async-start | bytes 655360 | tf_op jit(solution)/shard_map/all_to_all | solution.py:351
  20.9 1.3 %collective-permute-start = (bf16[4,512]{1,0:T(4,128)(2,1)S(1)}, bf16[4,512]{1,0:T(4,128)(2,1)S(1)}, u32[]{:S(2)}, u32[]{:S(2)}) collective-permute-start(bf16[4,512]{1,0:T(4,128)(2,1)S(1)} %copy-done), channel_id=1, source_target_pairs={{0,1},{1,0},{2,3},{3,2},{4,5},{5,4},{6,7},{7,6},{8,9},{9,8},{10,11... | collective-permute-start | bytes 12296 | tf_op jit(solution)/shard_map/ppermute | solution.py:333
  22.2 7.9 %copy-start.1 = (f32[256]{0:T(256)S(1)}, f32[256]{0:T(256)}, u32[]{:S(2)}) copy-start(f32[256]{0:T(256)} %param.11) | copy-start | bytes 3076
  22.2 7.9 %copy-start.2 = (bf16[4,256]{1,0:T(4,128)(2,1)S(1)}, bf16[4,256]{1,0:T(4,128)(2,1)}, u32[]{:S(2)}) copy-start(bf16[4,256]{1,0:T(4,128)(2,1)} %refs_7_.1) | copy-start | bytes 6148
  22.2 4.7 %collective-permute-start.1 = (bf16[2,4,512]{2,1,0:T(4,128)(2,1)S(1)}, bf16[2,4,512]{2,1,0:T(4,128)(2,1)S(1)}, u32[]{:S(2)}, u32[]{:S(2)}) collective-permute-start(bf16[2,4,512]{2,1,0:T(4,128)(2,1)S(1)} %pad_maximum_fusion), channel_id=1, source_target_pairs={{0,2},{1,3},{2,4},{3,5},{4,6},{5,7},{6,0},{7,1},{8,10},{9,11},{10,... | collective-permute-start | bytes 24584 | tf_op jit(solution)/shard_map/ppermute | solution.py:356
  22.7 5.2 %collective-permute-start.2 = (bf16[2,4,512]{2,1,0:T(4,128)(2,1)S(1)}, bf16[2,4,512]{2,1,0:T(4,128)(2,1)S(1)}, u32[]{:S(2)}, u32[]{:S(2)}) collective-permute-start(bf16[2,4,512]{2,1,0:T(4,128)(2,1)S(1)} %pad_maximum_fusion), channel_id=1, source_target_pairs={{0,4},{1,5},{2,6},{3,7},{4,0},{5,1},{6,2},{7,3},{8,12},{9,13},{10,... | collective-permute-start | bytes 24584 | tf_op jit(solution)/shard_map/ppermute | solution.py:356
  25.2 4.9 %collective-permute-start.3 = (bf16[2,4,512]{2,1,0:T(4,128)(2,1)S(1)}, bf16[2,4,512]{2,1,0:T(4,128)(2,1)S(1)}, u32[]{:S(2)}, u32[]{:S(2)}) collective-permute-start(bf16[2,4,512]{2,1,0:T(4,128)(2,1)S(1)} %pad_maximum_fusion), channel_id=1, source_target_pairs={{0,6},{1,7},{2,0},{3,1},{4,2},{5,3},{6,4},{7,5},{8,14},{9,15},{10,... | collective-permute-start | bytes 24584 | tf_op jit(solution)/shard_map/ppermute | solution.py:356
  30.0 22.9 %copy-start.3 = (f32[128]{0:T(128)S(1)}, f32[128]{0:T(128)}, u32[]{:S(2)}) copy-start(f32[128]{0:T(128)} %param.15) | copy-start | bytes 1540
